TPU v7x, 32 devices: a whole 2x2x4 slice. The times are simulated.
32 devices in a mesh: ep: 8 (over z, y), tp: 4 (over x, core).
Axes of the slice: x: 2, y: 2, z: 4, core: 2. Of those that a mesh axis runs over, the one named last changes fastest.
Arguments:
- query_rows: bfloat16 [1024, 1024], P('ep', 'tp'), may hold values from -10 to 10
- key_rows: bfloat16 [1024, 1024], P('ep', 'tp'), may hold values from -10 to 10
- value_rows: bfloat16 [1024, 1024], P('ep', 'tp'), may hold values from -6 to 6
- key_bias: bfloat16 [1024, 16], P('ep', 'tp'), may hold values from -24 to 4
- mixer_weight: bfloat16 [1024, 2048], P('tp'), may hold values from -0.1875 to 0.1875
- mixer_gain: float32 [2048], replicated, may hold values from 0.1 to 1.9
- routed_input: bfloat16 [3072, 2048], P(('ep', 'tp')), may hold values from -6 to 6
- entry_gain: float32 [2048], replicated, may hold values from 0.1 to 1.9
- expert_index: int32 [3072, 2], P(('ep', 'tp')), may hold values from 0 to 15, all different within a row; in each aligned block of 96 rows (0 to 95, 96 to 191, ...) at most 18 rows name the same one
- route_weights: float32 [3072, 2], P(('ep', 'tp')), may hold values from 0.1 to 1
- expert_gate: bfloat16 [16, 2048, 1024], P('ep', None, 'tp'), may hold values from -0.125 to 0.125
- expert_up: bfloat16 [16, 2048, 1024], P('ep', None, 'tp'), may hold values from -0.125 to 0.125
- expert_down: bfloat16 [16, 1024, 2048], P('ep', 'tp'), may hold values from -0.1875 to 0.1875
- shared_gate: bfloat16 [2048, 1024], P(None, 'tp'), may hold values from -0.125 to 0.125
- shared_up: bfloat16 [2048, 1024], P(None, 'tp'), may hold values from -0.125 to 0.125
- shared_down: bfloat16 [1024, 2048], P('tp'), may hold values from -0.1875 to 0.1875
- exit_gain: float32 [2048], replicated, may hold values from 0.1 to 1.9
Outputs:
- mixer_out: bfloat16 [1024, 2048], P(('ep', 'tp'))
- expert_out: bfloat16 [3072, 2048], P(('ep', 'tp'))
Inputs may be any that keep to these rules, and one draw needn't show every extreme that they name: `expert_index`: in each aligned block of 96 rows (the rows of one device) no expert is named by more than 18 rows, a bound that some block reaches; each row names 2 different experts.
All inputs are finite; a program needn't handle non-finite values.
Results may differ from a plain program's by a relative error of at most 0.012.
Values may be sent and summed in bfloat16 or wider, within the bound.
A program may use at most 128 MiB of HBM per device.

v0:
```python
import jax
import jax.numpy as jnp
from jax import lax
from jax.sharding import PartitionSpec as P

EPS = 1e-06


def root_norm(values, gain_row):
    return values * lax.rsqrt(jnp.mean(values * values, axis=-1, keepdims=True) + EPS) * gain_row


def rounded_term(partial_value):
    return lax.optimization_barrier(partial_value.astype(jnp.bfloat16)).astype(jnp.float32)


def block_shards(shard_rows, ep_size):
    shards = 1
    while shards * shard_rows < 512 and ep_size % (2 * shards) == 0:
        shards = shards * 2
    return shards


def break_scores(query_split, block_keys, block_bias, query_pos, key_start):
    head_count = query_split.shape[1]
    key_count = block_keys.shape[0]
    keys_split = block_keys.reshape(key_count, head_count, query_split.shape[2])
    scores = jnp.einsum("qhd,khd->hqk", query_split, keys_split, preferred_element_type=jnp.float32)
    scores = (
        scores * query_split.shape[2] ** (-0.5)
        + jnp.transpose(block_bias.astype(jnp.float32))[:, None, :]
    )
    key_pos = key_start + jnp.arange(key_count, dtype=jnp.int32)
    causal = (key_pos[None, :] < query_pos[:, None])[None]
    fail_logs = jnp.where(causal, -jax.nn.softplus(scores), 0.0)
    return (scores, fail_logs, causal)


def break_values(scores, fail_logs, causal, offset, block_values):
    later_sum = lax.cumsum(fail_logs, axis=2, reverse=True) - fail_logs + offset[:, :, None]
    weights = jnp.where(causal, jnp.exp(jax.nn.log_sigmoid(scores) + later_sum), 0.0).astype(
        jnp.bfloat16
    )
    values_split = block_values.reshape(block_values.shape[0], scores.shape[0], -1)
    return jnp.einsum("hqk,khd->qhd", weights, values_split, preferred_element_type=jnp.float32)


def shared_term_of(own_all, shared_gate, shared_up, shared_down):
    gate_part = jnp.dot(own_all, shared_gate, preferred_element_type=jnp.float32)
    up_part = jnp.dot(own_all, shared_up, preferred_element_type=jnp.float32)
    hidden = (jax.nn.silu(gate_part) * up_part).astype(jnp.bfloat16)
    return rounded_term(jnp.dot(hidden, shared_down, preferred_element_type=jnp.float32))


def on_device(
    query_rows,
    key_rows,
    value_rows,
    key_bias,
    mixer_weight,
    mixer_gain,
    routed_input,
    entry_gain,
    expert_index,
    route_weights,
    expert_gate,
    expert_up,
    expert_down,
    shared_gate,
    shared_up,
    shared_down,
    exit_gain,
):
    shard_rows = query_rows.shape[0]
    head_count = key_bias.shape[1]
    head_size = query_rows.shape[1] // head_count
    ep_size = lax.axis_size("ep")
    tp_size = lax.axis_size("tp")
    own_index = lax.axis_index("ep")
    query_split = query_rows.reshape(shard_rows, head_count, head_size)
    query_pos = own_index * shard_rows + jnp.arange(shard_rows, dtype=jnp.int32)
    span_shards = block_shards(shard_rows, ep_size)
    empty_output = jnp.zeros((shard_rows, head_count, head_size), jnp.float32)
    all_keys, all_values, all_bias = (
        lax.all_gather(key_rows, "ep", axis=0, tiled=True),
        lax.all_gather(value_rows, "ep", axis=0, tiled=True),
        lax.all_gather(key_bias, "ep", axis=0, tiled=True),
    )
    block_rows = span_shards * shard_rows
    own_block = own_index * shard_rows // block_rows

    def backward_turn(turn_index, carried_pair):
        output, carried = carried_pair
        block_start = (own_block - turn_index) * block_rows
        block_keys = lax.dynamic_slice_in_dim(all_keys, block_start, block_rows, 0)
        block_values = lax.dynamic_slice_in_dim(all_values, block_start, block_rows, 0)
        block_bias = lax.dynamic_slice_in_dim(all_bias, block_start, block_rows, 0)
        scores, fail_logs, causal = break_scores(
            query_split, block_keys, block_bias, query_pos, block_start
        )
        output = output + break_values(scores, fail_logs, causal, carried, block_values)
        return (output, carried + jnp.sum(fail_logs, axis=2))

    carried_zero = jnp.zeros((head_count, shard_rows), jnp.float32)
    output, unused = lax.fori_loop(0, own_block + 1, backward_turn, (empty_output, carried_zero))
    attended = output.reshape(shard_rows, head_count * head_size).astype(jnp.bfloat16)
    mixer_term = rounded_term(jnp.dot(attended, mixer_weight, preferred_element_type=jnp.float32))
    row_count = routed_input.shape[0]
    top_count = expert_index.shape[1]
    local_experts = expert_gate.shape[0]
    model_width = routed_input.shape[1]
    expert_count = local_experts * ep_size
    capacity = 3 * row_count * top_count // (2 * expert_count)
    slot_total = expert_count * capacity
    normed = root_norm(routed_input.astype(jnp.float32), entry_gain).astype(jnp.bfloat16)
    flat_expert = expert_index.reshape(-1)
    onehot = (flat_expert[:, None] == jnp.arange(expert_count, dtype=jnp.int32)[None, :]).astype(
        jnp.int32
    )
    slot_rank = jnp.sum((jnp.cumsum(onehot, axis=0) - onehot) * onehot, axis=1)
    slot_index = (flat_expert * capacity + slot_rank).reshape(row_count, top_count)
    matches = slot_index[None, :, :] == jnp.arange(slot_total, dtype=jnp.int32)[:, None, None]
    selector = jnp.any(matches, axis=2).astype(jnp.bfloat16)
    outgoing = jnp.dot(selector, normed, preferred_element_type=jnp.float32).astype(jnp.bfloat16)
    outgoing = outgoing.reshape(expert_count, capacity, model_width)
    arrived = lax.all_to_all(outgoing, "ep", split_axis=0, concat_axis=0, tiled=True)
    gate_all, up_all, down_all, own_all = (
        lax.all_gather(expert_gate, "tp", axis=2, tiled=True),
        lax.all_gather(expert_up, "tp", axis=2, tiled=True),
        lax.all_gather(expert_down, "tp", axis=1, tiled=True),
        lax.all_gather(normed, "tp", axis=0, tiled=True),
    )
    arrived_split = arrived.reshape(ep_size, local_experts, capacity, model_width)
    gate_part = jnp.einsum(
        "secd,edf->secf", arrived_split, gate_all, preferred_element_type=jnp.float32
    )
    up_part = jnp.einsum(
        "secd,edf->secf", arrived_split, up_all, preferred_element_type=jnp.float32
    )
    hidden = (jax.nn.silu(gate_part) * up_part).astype(jnp.bfloat16)
    part_width = hidden.shape[3] // tp_size
    hidden_split = hidden.reshape(ep_size, local_experts, capacity, tp_size, part_width)
    down_split = down_all.reshape(local_experts, tp_size, part_width, model_width)
    part_sums = jnp.einsum(
        "secpf,epfd->psecd", hidden_split, down_split, preferred_element_type=jnp.float32
    )
    routed_sum = jnp.sum(rounded_term(part_sums), axis=0)
    shared_term = shared_term_of(own_all, shared_gate, shared_up, shared_down)
    mixer_sum, shared_sum = (
        lax.psum_scatter(
            mixer_term.astype(jnp.bfloat16), "tp", scatter_dimension=0, tiled=True
        ).astype(jnp.float32),
        lax.psum_scatter(
            shared_term.astype(jnp.bfloat16), "tp", scatter_dimension=0, tiled=True
        ).astype(jnp.float32),
    )
    returned_rows = routed_sum.astype(jnp.bfloat16).reshape(expert_count, capacity, model_width)
    back_rows = lax.all_to_all(
        returned_rows, "ep", split_axis=0, concat_axis=0, tiled=True
    ).reshape(slot_total, model_width)
    gathered = back_rows[slot_index].astype(jnp.float32)
    routed = jnp.sum(route_weights[:, :, None] * gathered, axis=1)
    combined = routed + shared_sum
    expert_out = root_norm(combined, exit_gain).astype(jnp.bfloat16)
    mixer_out = root_norm(mixer_sum, mixer_gain).astype(jnp.bfloat16)
    return (mixer_out, expert_out)


def solution(mesh):
    in_specs = (
        P("ep", "tp"),
        P("ep", "tp"),
        P("ep", "tp"),
        P("ep", "tp"),
        P("tp", None),
        P(),
        P(("ep", "tp"), None),
        P(),
        P(("ep", "tp"), None),
        P(("ep", "tp"), None),
        P("ep", None, "tp"),
        P("ep", None, "tp"),
        P("ep", "tp", None),
        P(None, "tp"),
        P(None, "tp"),
        P("tp", None),
        P(),
    )
    out_specs = (P(("ep", "tp"), None), P(("ep", "tp"), None))
    return jax.shard_map(
        on_device, mesh=mesh, in_specs=in_specs, out_specs=out_specs, check_vma=False
    )
```

profile of v0, /device:TPU:0, one launch (start us, length us, event | category | flops | bytes accessed | tf_op | source)
XLA Modules:
  0.0 287.4 jit_solution(5951351913722797669)
XLA Ops:
  7.2 1.3 fusion.33
  8.5 1.9 fusion.35
  10.5 0.7 all-gather.5.cloned.1.call-update
  11.2 0.7 all-gather.7.cloned.1.call-update
  12.0 0.5 all-gather.9.cloned.1.call-update
  12.8 0.6 reduce-window.16
  13.4 0.2 slice_reduce_fusion
  13.7 0.1 reduce_sum.70
  14.0 0.5 convolution_convert_fusion.1
  14.5 1.4 reshape.127
  15.9 7.5 %all-to-all-start = ((bf16[16,18,2048]{2,1,0:T(8,128)(2,1)}), bf16[16,18,2048]{2,1,0:T(8,128)(2,1)}, u32[]{:S(2)}, u32[]{:S(2)}) async-start(bf16[16,18,2048]{2,1,0:T(8,128)(2,1)} %reshape.127), calls=%async_computation.1 | async-start | bytes 3145728 | tf_op jit(solution)/shard_map/all_to_all | solution.py:126
  23.7 0.7 copy.130
  24.4 39.9 %all_gather.23 = bf16[1024,4]{0,1:T(4,128)(2,1)S(1)} all-gather(bf16[128,4]{0,1:T(4,128)(2,1)S(1)} %copy-done.11), channel_id=1, replica_groups=mesh['ep'=8,'tp'=4] {'ep'}, dimensions={0}, use_global_device_ids=true | all-gather | bytes 9216 | tf_op jit(solution)/shard_map/all_gather | solution.py:87
  64.2 33.0 %all_gather.21 = bf16[1024,256]{0,1:T(8,128)(2,1)} all-gather(bf16[128,256]{0,1:T(8,128)(2,1)S(1)} %copy.128), channel_id=1, replica_groups=mesh['ep'=8,'tp'=4] {'ep'}, dimensions={0}, use_global_device_ids=true | all-gather | bytes 589824 | tf_op jit(solution)/shard_map/all_gather | solution.py:86
  97.2 28.8 %all_gather.22 = bf16[1024,256]{0,1:T(8,128)(2,1)} all-gather(bf16[128,256]{0,1:T(8,128)(2,1)S(1)} %copy.129), channel_id=1, replica_groups=mesh['ep'=8,'tp'=4] {'ep'}, dimensions={0}, use_global_device_ids=true | all-gather | bytes 589824 | tf_op jit(solution)/shard_map/all_gather | solution.py:85
  126.0 0.7 broadcast_in_dim.25
  126.7 10.7 %while.13 = (s32[]{:T(128)}, f32[128,4,64]{0,2,1:T(8,128)}, f32[4,128]{1,0:T(4,128)S(1)}, s32[]{:T(128)}, s32[]{:T(128)}, /*index=5*/bf16[1024,256]{0,1:T(8,128)...) while((s32[]{:T(128)}, f32[128,4,64]{0,2,1:T(8,128)}, ...), condition=%wide.region_4.5_spmd.clone, body=%wide.region_0.4_spmd.clone.sunk | while | flops 109160584 | bytes 14775571 | solution.py:105
  126.7 1.1 constant_dynamic-slice_fusion.3
  127.9 1.8 fusion.78
  129.7 4.8 %fusion.79 = f32[4,128,4,128]{1,2,3,0:T(4,128)S(1)} fusion(f32[4,128,4,128]{1,3,2,0:T(8,128)S(1)} %bitcast.106), kind=kOutput, calls=%fused_computation.18.clone.1 | output fusion | flops 33292288 | bytes 2097152 | tf_op jit(solution)/shard_map/reduce-window
  134.6 0.2 broadcast_add_fusion.2
  134.9 1.5 fusion.80
  136.4 0.2 fusion.81
  136.7 0.6 copy-done.3
  137.3 0.9 convert_element_type.63
  138.3 2.4 convolution_convert_fusion.2
  140.7 0.2 reduce-scatter.5.cloned.1.call-start
  141.0 2.4 fusion.50
  143.4 4.2 %convolution_convert_fusion = bf16[384,2048]{1,0:T(8,128)(2,1)} fusion(bf16[256,2048]{1,0:T(8,128)(2,1)S(1)} %copy-done, bf16[384,2048]{1,0:T(8,128)(2,1)S(1)} %copy-done.13, bf16[2048,256]{1,0:T(8,128)(2,1)} %param.33, f32[384,256]{1,0:T(8,128)S(1)} %fusion.50), kind=kOutput, calls=%fused_computation.36 | convolution fusion | flops 806682624 | bytes 5636096 | tf_op jit(solution)/shard_map/dot_general | solution.py:52
  147.6 5.7 %fusion.18 = f32[2,8,18,1024]{3,2,1,0:T(8,128)S(1)} fusion(bf16[2,2048,1024]{2,1,0:T(8,128)(2,1)} %all-gather.5.cloned.1.call-done, bf16[8,2,18,2048]{3,2,1,0:T(8,128)(2,1)} %bitcast.3), kind=kOutput, calls=%fused_computation.31 | convolution fusion | flops 1207959552 | bytes 10747904 | tf_op jit(solution)/shard_map/secd,edf->secf/dot_general | solution.py:134
  153.3 1.6 all-gather.7.cloned.1.call-done
  154.9 5.8 %fusion.24 = bf16[8,2,18,1024]{3,2,0,1:T(8,128)(2,1)S(1)} fusion(f32[2,8,18,1024]{3,2,1,0:T(8,128)S(1)} %fusion.18, bf16[2,2048,1024]{2,1,0:T(8,128)(2,1)} %all-gather.7.cloned.1.call-done, bf16[8,2,18,2048]{3,2,1,0:T(8,128)(2,1)} %bitcast.3), kind=kOutput, calls=%fused_computation.40 | convolution fusion | flops 1209729024 | bytes 11337728 | tf_op jit(solution)/shard_map/secd,edf->secf/dot_general | solution.py:137
  160.7 0.3 reshape.152
  161.1 53.5 %all-gather.9.cloned.1.call-done = bf16[2,1024,2048]{2,1,0:T(8,128)(2,1)} async-done(((bf16[2,256,2048]{2,1,0:T(8,128)(2,1)}), bf16[2,1024,2048]{2,1,0:T(8,128)(2,1)}) %all-gather.9.cloned.1.call-update) | async-done | bytes 8388624 | tf_op jit(solution)/shard_map/all_gather | solution.py:130
  214.6 7.9 %convert_bitcast_fusion.1 = bf16[4,8,2,18,2048]{4,3,1,2,0:T(8,128)(2,1)} fusion(bf16[2,4,256,2048,1]{3,2,1,0,4:T(8,128)(2,1)} %bitcast.108, bf16[8,2,18,4,256]{4,3,2,0,1:T(4,128)(2,1)S(1)} %reshape.152), kind=kOutput, calls=%fused_computation.35 | convolution fusion | flops 1210318848 | bytes 13697024 | tf_op jit(solution)/shard_map/secpf,epfd->psecd/dot_general | solution.py:144
  222.5 4.5 %reduce_sum.72 = bf16[8,2,18,2048]{3,2,0,1:T(8,128)(2,1)S(1)} reduce(bf16[4,8,2,18,2048]{4,3,1,2,0:T(8,128)(2,1)} %convert_bitcast_fusion.1, bf16[]{:T(256)} %constant.74.clone.1), dimensions={0}, to_apply=%region_12.13 | reduce | flops 1769472 | bytes 5898242 | tf_op jit(solution)/shard_map/reduce_sum | solution.py:147
  227.0 1.2 copy.156
  228.2 5.6 %all-to-all-start.1 = ((bf16[16,18,2048]{2,1,0:T(8,128)(2,1)}), bf16[16,18,2048]{2,1,0:T(8,128)(2,1)}, u32[]{:S(2)}, u32[]{:S(2)}) async-start(bf16[16,18,2048]{2,1,0:T(8,128)(2,1)} %bitcast.13), calls=%async_computation.2 | async-start | bytes 3145728 | tf_op jit(solution)/shard_map/all_to_all | solution.py:158
  234.2 4.4 %reduce-scatter.3.cloned.1.call-done = bf16[32,2048]{1,0:T(8,128)(2,1)} async-done(((bf16[128,2048]{1,0:T(8,128)(2,1)}), bf16[32,2048]{1,0:T(8,128)(2,1)}) %reduce-scatter.3.cloned.1.call-update) | async-done | bytes 131088 | tf_op jit(solution)/shard_map/reduce_scatter | solution.py:150
  238.6 1.0 fusion.43
  239.7 1.7 fusion.45
  241.3 30.1 %all-to-all-done.1 = bf16[16,18,2048]{2,1,0:T(8,128)(2,1)} async-done(((bf16[16,18,2048]{2,1,0:T(8,128)(2,1)}), bf16[16,18,2048]{2,1,0:T(8,128)(2,1)}, u32[]{:S(2)}, u32[]{:S(2)}) %all-to-all-start.1) | async-done | bytes 1179680 | tf_op jit(solution)/shard_map/all_to_all | solution.py:158
  271.4 1.6 reshape.132
  273.0 1.1 gather_fusion
  274.1 1.0 reshape.144
  275.1 2.3 multiply_reduce_fusion
  277.4 1.2 multiply_reduce_fusion.1
  278.7 1.9 multiply_convert_fusion
  (69 shorter events, 1.8 us)
Async XLA Ops:
  7.2 136.2 %copy-start = (bf16[256,2048]{1,0:T(8,128)(2,1)S(1)}, bf16[256,2048]{1,0:T(8,128)(2,1)}, u32[]{:S(2)}) copy-start(bf16[256,2048]{1,0:T(8,128)(2,1)} %param.34) | copy-start | bytes 3145732
  7.2 133.8 %all-gather.11.cloned.1.call-start = ((), (), s32[]{:S(2)}) async-start(), calls=%async_computation.8 | async-start | bytes 1966080 | tf_op jit(solution)/shard_map/all_gather | solution.py:131
  10.4 137.2 %all-gather.5.cloned.1.call-start = ((), (), s32[]{:S(2)}) async-start(), calls=%async_computation.5 | async-start | bytes 10485760 | tf_op jit(solution)/shard_map/all_gather | solution.py:128
  11.2 1.3 copy-start.10
  11.2 143.7 %all-gather.7.cloned.1.call-start = ((), (), s32[]{:S(2)}) async-start(), calls=%async_computation.6 | async-start | bytes 10485760 | tf_op jit(solution)/shard_map/all_gather | solution.py:129
  11.9 2.1 copy-start.4
  11.9 202.6 %all-gather.9.cloned.1.call-start = ((), (), s32[]{:S(2)}) async-start(), calls=%async_computation.7 | async-start | bytes 10485760 | tf_op jit(solution)/shard_map/all_gather | solution.py:130
  15.9 7.5 %copy-start.5 = (bf16[128,256]{1,0:T(8,128)(2,1)S(1)}, bf16[128,256]{1,0:T(8,128)(2,1)}, u32[]{:S(2)}) copy-start(bf16[128,256]{1,0:T(8,128)(2,1)} %param.21) | copy-start | bytes 196612
  15.9 7.7 %copy-start.6 = (bf16[128,256]{1,0:T(8,128)(2,1)S(1)}, bf16[128,256]{1,0:T(8,128)(2,1)}, u32[]{:S(2)}) copy-start(bf16[128,256]{1,0:T(8,128)(2,1)} %param.20) | copy-start | bytes 196612
  15.9 7.8 %copy-start.7 = (bf16[128,256]{1,0:T(8,128)(2,1)S(1)}, bf16[128,256]{1,0:T(8,128)(2,1)}, u32[]{:S(2)}) copy-start(bf16[128,256]{1,0:T(8,128)(2,1)} %param.19) | copy-start | bytes 196612
  15.9 8.5 %copy-start.11 = (bf16[128,4]{0,1:T(4,128)(2,1)S(1)}, bf16[128,4]{0,1:T(4,128)(2,1)}, u32[]{:S(2)}) copy-start(bf16[128,4]{0,1:T(4,128)(2,1)} %param.22) | copy-start | bytes 3076
  15.9 131.7 %all-to-all-start = ((bf16[16,18,2048]{2,1,0:T(8,128)(2,1)}), bf16[16,18,2048]{2,1,0:T(8,128)(2,1)}, u32[]{:S(2)}, u32[]{:S(2)}) async-start(bf16[16,18,2048]{2,1,0:T(8,128)(2,1)} %reshape.127), calls=%async_computation.1 | async-start | bytes 3145728 | tf_op jit(solution)/shard_map/all_to_all | solution.py:126
  23.3 215.3 %reduce-scatter.3.cloned.1.call-start = ((), (), s32[]{:S(2)}) async-start(), calls=%async_computation.4 | async-start | bytes 655360 | tf_op jit(solution)/shard_map/reduce_scatter | solution.py:150
  134.9 1.5 copy-start.2
  136.7 0.7 copy-start.3
  140.7 136.7 %reduce-scatter.5.cloned.1.call-start = ((), (), s32[]{:S(2)}) async-start(), calls=%async_computation.9 | async-start | bytes 1966080 | tf_op jit(solution)/shard_map/reduce_scatter | solution.py:153
  140.9 2.4 copy-start.13
  228.2 5.9 %copy-start.12 = (f32[96,2]{0,1:T(2,128)S(1)}, f32[96,2]{0,1:T(2,128)}, u32[]{:S(2)}) copy-start(f32[96,2]{0,1:T(2,128)} %param.28) | copy-start | bytes 2308
  228.2 11.4 %copy-start.9 = (f32[2048]{0:T(1024)S(1)}, f32[2048]{0:T(1024)}, u32[]{:S(2)}) copy-start(f32[2048]{0:T(1024)} %param.24) | copy-start | bytes 24580
  228.2 43.2 %all-to-all-start.1 = ((bf16[16,18,2048]{2,1,0:T(8,128)(2,1)}), bf16[16,18,2048]{2,1,0:T(8,128)(2,1)}, u32[]{:S(2)}, u32[]{:S(2)}) async-start(bf16[16,18,2048]{2,1,0:T(8,128)(2,1)} %bitcast.13), calls=%async_computation.2 | async-start | bytes 3145728 | tf_op jit(solution)/shard_map/all_to_all | solution.py:158
  275.1 3.6 %copy-start.8 = (f32[2048]{0:T(1024)S(1)}, f32[2048]{0:T(1024)}, u32[]{:S(2)}) copy-start(f32[2048]{0:T(1024)} %param.35) | copy-start | bytes 24580
  275.1 5.5 %copy-start.1 = (bf16[256,2048]{1,0:T(8,128)(2,1)S(1)}, bf16[256,2048]{1,0:T(8,128)(2,1)}, u32[]{:S(2)}) copy-start(bf16[256,2048]{1,0:T(8,128)(2,1)} %param.34) | copy-start | bytes 3145732
Sparse Core Ops, SparseCore 0:
  10.6 22.3 all-gather.10
  34.5 59.3 all-gather.4
  95.5 59.3 all-gather.6
  156.3 58.2 all-gather.8
  216.9 21.6 reduce-scatter.2
  241.0 27.9 reduce-scatter.4
where the time goes:
time: 288 us; the launch traced here: 287 us
  blocking collectives  102 us (35%)
  waiting for transfers between devices  91.6 us (32%)
  matrix products  30.9 us (11%)
  other arithmetic  24.1 us (8%)
  between operations  14.4 us (5%)
  starting transfers between devices  13.5 us (5%)
  local copies, waits for them, and re-layouts  11.1 us (4%)
    all_gather x1, waiting for transfers between devices, on_device(): lax.all_gather(expert_down, 'tp', axis=1, tiled=True)  53.5 us
    all_gather x1, blocking collectives, on_device(): lax.all_gather(key_bias, 'ep', axis=0, tiled=True)  39.9 us
    all_gather x1, blocking collectives, on_device(): lax.all_gather(value_rows, 'ep', axis=0, tiled=True)  33 us
    all_to_all x1, waiting for transfers between devices, on_device(): lax.all_to_all(returned_rows, 'ep', split_axis=0, concat_axis=0, tiled=True)  30.1 us
    all_gather x1, blocking collectives, on_device(): lax.all_gather(key_rows, 'ep', axis=0, tiled=True)  28.8 us
    dot_general x1, matrix products, on_device(): jnp.einsum('secpf,epfd->psecd', hidden_split, down_split, preferred_eleme...  7.91 us
    all_to_all x1, starting transfers between devices, on_device(): lax.all_to_all(outgoing, 'ep', split_axis=0, concat_axis=0, tiled=True)  7.45 us
    dot_general x1, matrix products, on_device(): jnp.einsum('secd,edf->secf', arrived_split, up_all, preferred_element_typ...  5.82 us
  transfers between devices with their start and end apart: 8, of which 4 were waited for; matrix products, arithmetic and copies ran while one was open for 21% of the time, Pallas kernels for 0%

commit v1 on v0

v1 whole, which is shorter than its diff:
```python
import functools

import jax
import jax.numpy as jnp
from jax import lax
from jax.experimental import pallas as pl
from jax.experimental.pallas import tpu as pltpu
from jax.sharding import PartitionSpec as P

MESH = pl.DeviceIdType.MESH


def peer_places(ep_size, tp_size):
    own_ep = lax.axis_index("ep")
    own_tp = lax.axis_index("tp")
    partner = own_tp + 1 - 2 * lax.rem(own_tp, 2)
    across = lax.rem(own_tp + tp_size // 2, tp_size)
    return own_ep, own_tp, partner, across


def greet(ep_size, own_ep, own_tp, partner, across):
    barrier = pltpu.get_barrier_semaphore()

    def signal_one(step, unused):
        place = lax.rem(own_ep + step, ep_size)
        pl.semaphore_signal(barrier, inc=1, device_id=(place, own_tp), device_id_type=MESH)
        return unused

    lax.fori_loop(1, ep_size, signal_one, 0)
    for place in (partner, across):
        pl.semaphore_signal(barrier, inc=1, device_id=(own_ep, place), device_id_type=MESH)
    pl.semaphore_wait(barrier, ep_size + 1)


def send_of(source, target, send_sem, recv_sem, place):
    return pltpu.make_async_remote_copy(
        src_ref=source,
        dst_ref=target,
        send_sem=send_sem,
        recv_sem=recv_sem,
        device_id=place,
        device_id_type=MESH,
    )


def front_kernel(
    ep_size,
    tp_size,
    kv_ref,
    bias_ref,
    normed_ref,
    outgoing_ref,
    kv_all,
    bias_all,
    own_all,
    arrived,
    ep_send,
    ep_recv,
    kv_send,
    kv_recv,
    bias_send,
    bias_recv,
    partner_send,
    partner_recv,
    across_send,
    across_recv,
    relay_send,
    relay_recv,
    local_sem,
):
    own_ep, own_tp, partner, across = peer_places(ep_size, tp_size)
    greet(ep_size, own_ep, own_tp, partner, across)
    to_partner = (own_ep, partner)
    to_across = (own_ep, across)

    def dispatch(step):
        target = lax.rem(own_ep + step, ep_size)
        return send_of(
            outgoing_ref.at[target],
            arrived.at[own_tp, own_ep],
            ep_send.at[step],
            ep_recv.at[step],
            (target, own_tp),
        )

    def landed(step):
        source = lax.rem(own_ep - step + ep_size, ep_size)
        block = arrived.at[own_tp, source]
        return send_of(block, block, ep_send.at[step], ep_recv.at[step], (own_ep, own_tp))

    def spread_kv(step):
        target = lax.rem(own_ep + step, ep_size)
        return send_of(
            kv_ref, kv_all.at[own_ep], kv_send.at[step], kv_recv.at[step], (target, own_tp)
        )

    def landed_kv(step):
        block = kv_all.at[lax.rem(own_ep - step + ep_size, ep_size)]
        return send_of(block, block, kv_send.at[step], kv_recv.at[step], (own_ep, own_tp))

    def spread_bias(step):
        target = lax.rem(own_ep + step, ep_size)
        return send_of(
            bias_ref, bias_all.at[own_ep], bias_send.at[step], bias_recv.at[step], (target, own_tp)
        )

    def landed_bias(step):
        block = bias_all.at[lax.rem(own_ep - step + ep_size, ep_size)]
        return send_of(block, block, bias_send.at[step], bias_recv.at[step], (own_ep, own_tp))

    def tp_block(holder, step):
        return arrived.at[holder, lax.rem(own_ep - step + ep_size, ep_size)]

    def tp_copy(source, target, sems, step, place):
        return send_of(source, target, sems[0].at[step], sems[1].at[step], place)

    partner_sems = (partner_send, partner_recv)
    across_sems = (across_send, across_recv)
    relay_sems = (relay_send, relay_recv)
    last = ep_size

    lax.fori_loop(1, ep_size, lambda step, c: (dispatch(step).start(), c)[1], 0)
    own_block = outgoing_ref.at[own_ep]
    own_slot = arrived.at[own_tp, own_ep]
    tp_copy(normed_ref, own_all.at[own_tp], across_sems, last, to_across).start()
    tp_copy(own_block, own_slot, across_sems, 0, to_across).start()
    tp_copy(normed_ref, own_all.at[own_tp], partner_sems, last, to_partner).start()
    tp_copy(own_block, own_slot, partner_sems, 0, to_partner).start()
    locals_ = [
        pltpu.make_async_copy(own_block, own_slot, local_sem.at[0]),
        pltpu.make_async_copy(normed_ref, own_all.at[own_tp], local_sem.at[1]),
        pltpu.make_async_copy(kv_ref, kv_all.at[own_ep], local_sem.at[2]),
        pltpu.make_async_copy(bias_ref, bias_all.at[own_ep], local_sem.at[3]),
    ]
    for local in locals_:
        local.start()

    def start_kv(step, carry):
        spread_kv(step).start()
        spread_bias(step).start()
        return carry

    lax.fori_loop(1, ep_size, start_kv, 0)

    def forward(step, carry):
        landed(step).wait_recv()
        block = tp_block(own_tp, step)
        tp_copy(block, block, across_sems, step, to_across).start()
        tp_copy(block, block, partner_sems, step, to_partner).start()
        return carry

    lax.fori_loop(1, ep_size, forward, 0)

    other_own = own_all.at[across]
    tp_copy(other_own, other_own, across_sems, last, to_across).wait_recv()
    tp_copy(other_own, other_own, relay_sems, last, to_partner).start()

    def relay(step, carry):
        block = tp_block(across, step)
        tp_copy(block, block, across_sems, step, to_across).wait_recv()
        tp_copy(block, block, relay_sems, step, to_partner).start()
        return carry

    lax.fori_loop(0, ep_size, relay, 0)

    diagonal = lax.rem(partner + tp_size // 2, tp_size)

    def finish(step, carry):
        near = tp_block(partner, step)
        far = tp_block(diagonal, step)
        tp_copy(near, near, partner_sems, step, to_partner).wait()
        tp_copy(far, far, relay_sems, step, to_partner).wait()
        tp_copy(near, near, across_sems, step, to_across).wait_send()
        return carry

    lax.fori_loop(0, ep_size, finish, 0)
    near = own_all.at[partner]
    far = own_all.at[diagonal]
    tp_copy(near, near, partner_sems, last, to_partner).wait()
    tp_copy(far, far, relay_sems, last, to_partner).wait()
    tp_copy(near, near, across_sems, last, to_across).wait_send()

    def finish_ep(step, carry):
        dispatch(step).wait_send()
        spread_kv(step).wait_send()
        spread_bias(step).wait_send()
        landed_kv(step).wait_recv()
        landed_bias(step).wait_recv()
        return carry

    lax.fori_loop(1, ep_size, finish_ep, 0)
    for local in locals_:
        local.wait()


def front_exchange(ep_size, tp_size, kv, bias, normed, outgoing):
    def spread(count, value):
        return jax.ShapeDtypeStruct((count,) + value.shape, value.dtype)

    ep_sem = pltpu.SemaphoreType.DMA((ep_size,))
    tp_sem = pltpu.SemaphoreType.DMA((ep_size + 1,))
    return pl.pallas_call(
        functools.partial(front_kernel, ep_size, tp_size),
        out_shape=(
            spread(ep_size, kv),
            spread(ep_size, bias),
            spread(tp_size, normed),
            spread(tp_size, outgoing),
        ),
        in_specs=[pl.BlockSpec(memory_space=pltpu.VMEM)] * 4,
        out_specs=[pl.BlockSpec(memory_space=pl.ANY)] * 4,
        scratch_shapes=[ep_sem] * 6 + [tp_sem] * 6 + [pltpu.SemaphoreType.DMA((4,))],
        compiler_params=pltpu.CompilerParams(collective_id=0, has_side_effects=True),
        name="front_exchange",
    )(kv, bias, normed, outgoing)


def back_kernel(
    ep_size,
    tp_size,
    part_ref,
    shared_ref,
    mixer_ref,
    back_ref,
    shared_out,
    mixer_out,
    near_in,
    near_shared,
    near_mixer,
    far_out,
    far_in,
    far_shared_out,
    far_shared,
    far_mixer_out,
    far_mixer,
    total,
    near_send,
    near_recv,
    far_send,
    far_recv,
    ep_send,
    ep_recv,
    local_sem,
):
    own_ep, own_tp, partner, across = peer_places(ep_size, tp_size)
    diagonal = lax.rem(partner + tp_size // 2, tp_size)
    greet(ep_size, own_ep, own_tp, partner, across)
    to_partner = (own_ep, partner)
    to_across = (own_ep, across)
    homes = (diagonal, partner)

    def place_of(step):
        return lax.rem(own_ep + 1 + step, ep_size)

    def near_copy(side, step):
        place = place_of(step)
        return send_of(
            part_ref.at[homes[side], place],
            near_in.at[side, place],
            near_send.at[side, step],
            near_recv.at[side, step],
            to_partner,
        )

    def near_small(side, source, target, slot):
        return send_of(
            source.at[homes[side]],
            target.at[side],
            near_send.at[side, slot],
            near_recv.at[side, slot],
            to_partner,
        )

    def far_copy(source, target, slot):
        return send_of(source, target, far_send.at[slot], far_recv.at[slot], to_across)

    shared_slot, mixer_slot = ep_size, ep_size + 1

    for side in range(2):
        lax.fori_loop(
            0, ep_size, lambda step, c, side=side: (near_copy(side, step).start(), c)[1], 0
        )
        near_small(side, shared_ref, near_shared, shared_slot).start()
        near_small(side, mixer_ref, near_mixer, mixer_slot).start()

    def add(left, right):
        return left.astype(jnp.float32) + right.astype(jnp.float32)

    def pass_on(step, carry):
        place = place_of(step)
        near_copy(0, step).wait_recv()
        far_out[place] = add(part_ref[across, place], near_in[0, place]).astype(jnp.bfloat16)
        far_copy(far_out.at[place], far_in.at[place], step).start()
        return carry

    lax.fori_loop(0, ep_size, pass_on, 0)
    near_small(0, shared_ref, near_shared, shared_slot).wait_recv()
    far_shared_out[...] = add(shared_ref[across], near_shared[0]).astype(jnp.bfloat16)
    far_copy(far_shared_out, far_shared, shared_slot).start()
    near_small(0, mixer_ref, near_mixer, mixer_slot).wait_recv()
    far_mixer_out[...] = add(mixer_ref[across], near_mixer[0]).astype(jnp.bfloat16)
    far_copy(far_mixer_out, far_mixer, mixer_slot).start()

    def send_back(step):
        place = place_of(step)
        return send_of(
            total.at[place],
            back_ref.at[own_ep],
            ep_send.at[step],
            ep_recv.at[step],
            (place, own_tp),
        )

    def gather_total(step):
        place = place_of(step)
        near_copy(1, step).wait_recv()
        far_copy(far_out.at[place], far_in.at[place], step).wait_recv()
        value = add(part_ref[own_tp, place], near_in[1, place]) + far_in[place].astype(jnp.float32)
        total[place] = value.astype(jnp.bfloat16)

    def return_one(step, carry):
        gather_total(step)
        send_back(step).start()
        return carry

    lax.fori_loop(0, ep_size - 1, return_one, 0)
    gather_total(ep_size - 1)
    local = pltpu.make_async_copy(total.at[own_ep], back_ref.at[own_ep], local_sem)
    local.start()

    near_small(1, shared_ref, near_shared, shared_slot).wait_recv()
    far_copy(far_shared_out, far_shared, shared_slot).wait_recv()
    shared_out[...] = add(shared_ref[own_tp], near_shared[1]) + far_shared[...].astype(jnp.float32)
    near_small(1, mixer_ref, near_mixer, mixer_slot).wait_recv()
    far_copy(far_mixer_out, far_mixer, mixer_slot).wait_recv()
    mixer_out[...] = add(mixer_ref[own_tp], near_mixer[1]) + far_mixer[...].astype(jnp.float32)

    def finish(step, carry):
        place = place_of(step)
        near_copy(0, step).wait_send()
        near_copy(1, step).wait_send()
        far_copy(far_out.at[place], far_in.at[place], step).wait_send()
        return carry

    lax.fori_loop(0, ep_size, finish, 0)
    for side in range(2):
        near_small(side, shared_ref, near_shared, shared_slot).wait_send()
        near_small(side, mixer_ref, near_mixer, mixer_slot).wait_send()
    far_copy(far_shared_out, far_shared, shared_slot).wait_send()
    far_copy(far_mixer_out, far_mixer, mixer_slot).wait_send()

    def finish_ep(step, carry):
        send_back(step).wait_send()
        source = lax.rem(own_ep - 1 - step + 2 * ep_size, ep_size)
        block = back_ref.at[source]
        send_of(
            block, block, ep_send.at[step], ep_recv.at[step], (own_ep, own_tp)
        ).wait_recv()
        return carry

    lax.fori_loop(0, ep_size - 1, finish_ep, 0)
    local.wait()


def back_exchange(ep_size, tp_size, part, shared, mixer):
    block = part.shape[2:]
    bf16 = jnp.bfloat16
    sem = pltpu.SemaphoreType.DMA
    vmem = pl.BlockSpec(memory_space=pltpu.VMEM)
    return pl.pallas_call(
        functools.partial(back_kernel, ep_size, tp_size),
        out_shape=(
            jax.ShapeDtypeStruct((ep_size,) + block, bf16),
            jax.ShapeDtypeStruct(shared.shape[1:], jnp.float32),
            jax.ShapeDtypeStruct(mixer.shape[1:], jnp.float32),
        ),
        in_specs=[vmem] * 3,
        out_specs=[pl.BlockSpec(memory_space=pl.ANY), vmem, vmem],
        scratch_shapes=[
            pltpu.VMEM((2, ep_size) + block, bf16),
            pltpu.VMEM((2,) + shared.shape[1:], bf16),
            pltpu.VMEM((2,) + mixer.shape[1:], bf16),
            pltpu.VMEM((ep_size,) + block, bf16),
            pltpu.VMEM((ep_size,) + block, bf16),
            pltpu.VMEM(shared.shape[1:], bf16),
            pltpu.VMEM(shared.shape[1:], bf16),
            pltpu.VMEM(mixer.shape[1:], bf16),
            pltpu.VMEM(mixer.shape[1:], bf16),
            pltpu.VMEM((ep_size,) + block, bf16),
            sem((2, ep_size + 2)),
            sem((2, ep_size + 2)),
            sem((ep_size + 2,)),
            sem((ep_size + 2,)),
            sem((ep_size,)),
            sem((ep_size,)),
            sem,
        ],
        compiler_params=pltpu.CompilerParams(
            collective_id=1, has_side_effects=True, vmem_limit_bytes=60 * 1024 * 1024
        ),
        name="back_exchange",
    )(part, shared, mixer)


EPS = 1e-06


def root_norm(values, gain_row):
    return values * lax.rsqrt(jnp.mean(values * values, axis=-1, keepdims=True) + EPS) * gain_row


def block_shards(shard_rows, ep_size):
    shards = 1
    while shards * shard_rows < 512 and ep_size % (2 * shards) == 0:
        shards = shards * 2
    return shards


def break_scores(query_split, block_keys, block_bias, query_pos, key_start):
    head_count = query_split.shape[1]
    key_count = block_keys.shape[0]
    keys_split = block_keys.reshape(key_count, head_count, query_split.shape[2])
    scores = jnp.einsum("qhd,khd->hqk", query_split, keys_split, preferred_element_type=jnp.float32)
    scores = (
        scores * query_split.shape[2] ** (-0.5)
        + jnp.transpose(block_bias.astype(jnp.float32))[:, None, :]
    )
    key_pos = key_start + jnp.arange(key_count, dtype=jnp.int32)
    causal = (key_pos[None, :] < query_pos[:, None])[None]
    fail_logs = jnp.where(causal, -jax.nn.softplus(scores), 0.0)
    return (scores, fail_logs, causal)


def break_values(scores, fail_logs, causal, offset, block_values):
    later_sum = lax.cumsum(fail_logs, axis=2, reverse=True) - fail_logs + offset[:, :, None]
    weights = jnp.where(causal, jnp.exp(jax.nn.log_sigmoid(scores) + later_sum), 0.0).astype(
        jnp.bfloat16
    )
    values_split = block_values.reshape(block_values.shape[0], scores.shape[0], -1)
    return jnp.einsum("hqk,khd->qhd", weights, values_split, preferred_element_type=jnp.float32)


def shared_term_of(own_all, shared_gate, shared_up, shared_down):
    gate_part = jnp.dot(own_all, shared_gate, preferred_element_type=jnp.float32)
    up_part = jnp.dot(own_all, shared_up, preferred_element_type=jnp.float32)
    hidden = (jax.nn.silu(gate_part) * up_part).astype(jnp.bfloat16)
    return jnp.dot(hidden, shared_down, preferred_element_type=jnp.float32).astype(jnp.bfloat16)


def on_device(
    query_rows,
    key_rows,
    value_rows,
    key_bias,
    mixer_weight,
    mixer_gain,
    routed_input,
    entry_gain,
    expert_index,
    route_weights,
    expert_gate,
    expert_up,
    expert_down,
    shared_gate,
    shared_up,
    shared_down,
    exit_gain,
):
    shard_rows = query_rows.shape[0]
    head_count = key_bias.shape[1]
    head_size = query_rows.shape[1] // head_count
    ep_size = lax.axis_size("ep")
    tp_size = lax.axis_size("tp")
    own_index = lax.axis_index("ep")
    query_split = query_rows.reshape(shard_rows, head_count, head_size)
    query_pos = own_index * shard_rows + jnp.arange(shard_rows, dtype=jnp.int32)
    span_shards = block_shards(shard_rows, ep_size)
    empty_output = jnp.zeros((shard_rows, head_count, head_size), jnp.float32)
    row_count = routed_input.shape[0]
    local_experts = expert_gate.shape[0]
    model_width = routed_input.shape[1]
    expert_count = local_experts * ep_size
    top_count = expert_index.shape[1]
    capacity = 3 * row_count * top_count // (2 * expert_count)
    block_slots = -(-local_experts * capacity // 16) * 16
    slot_total = ep_size * block_slots
    normed = root_norm(routed_input.astype(jnp.float32), entry_gain).astype(jnp.bfloat16)
    flat_expert = expert_index.reshape(-1)
    onehot = (flat_expert[:, None] == jnp.arange(expert_count, dtype=jnp.int32)[None, :]).astype(
        jnp.int32
    )
    slot_rank = jnp.sum((jnp.cumsum(onehot, axis=0) - onehot) * onehot, axis=1)
    slot_index = (
        flat_expert // local_experts * block_slots
        + flat_expert % local_experts * capacity
        + slot_rank
    ).reshape(row_count, top_count)
    slots = jnp.arange(slot_total, dtype=jnp.int32)
    matches = slot_index[None, :, :] == slots[:, None, None]
    selector = jnp.any(matches, axis=2).astype(jnp.bfloat16)
    outgoing = jnp.dot(selector, normed, preferred_element_type=jnp.float32).astype(jnp.bfloat16)
    outgoing = outgoing.reshape(ep_size, block_slots, model_width)
    bias_rows = -(-head_count // 16) * 16
    bias_block = jnp.pad(jnp.transpose(key_bias), ((0, bias_rows - head_count), (0, 0)))
    kv_block = jnp.concatenate([key_rows, value_rows], axis=1)
    kv_all, bias_all, own_all, arrived = front_exchange(
        ep_size, tp_size, kv_block, bias_block, normed, outgoing
    )
    width = key_rows.shape[1]
    all_keys = kv_all[:, :, :width].reshape(ep_size * shard_rows, width)
    all_values = kv_all[:, :, width:].reshape(ep_size * shard_rows, width)
    all_bias = jnp.swapaxes(bias_all[:, :head_count, :], 1, 2).reshape(
        ep_size * shard_rows, head_count
    )
    own_all = own_all.reshape(tp_size * row_count, model_width)
    block_rows = span_shards * shard_rows
    own_block = own_index * shard_rows // block_rows

    def backward_turn(turn_index, carried_pair):
        output, carried = carried_pair
        block_start = (own_block - turn_index) * block_rows
        block_keys = lax.dynamic_slice_in_dim(all_keys, block_start, block_rows, 0)
        block_values = lax.dynamic_slice_in_dim(all_values, block_start, block_rows, 0)
        block_bias = lax.dynamic_slice_in_dim(all_bias, block_start, block_rows, 0)
        scores, fail_logs, causal = break_scores(
            query_split, block_keys, block_bias, query_pos, block_start
        )
        output = output + break_values(scores, fail_logs, causal, carried, block_values)
        return (output, carried + jnp.sum(fail_logs, axis=2))

    carried_zero = jnp.zeros((head_count, shard_rows), jnp.float32)
    output, unused = lax.fori_loop(0, own_block + 1, backward_turn, (empty_output, carried_zero))
    attended = output.reshape(shard_rows, head_count * head_size).astype(jnp.bfloat16)
    mixer_term = jnp.dot(attended, mixer_weight, preferred_element_type=jnp.float32).astype(
        jnp.bfloat16
    )
    rows = arrived.reshape(tp_size * slot_total, model_width)
    row_expert = jnp.arange(tp_size * slot_total, dtype=jnp.int32) % block_slots // capacity
    pieces = []
    for expert in range(local_experts):
        gate_part = jnp.dot(rows, expert_gate[expert], preferred_element_type=jnp.float32)
        up_part = jnp.dot(rows, expert_up[expert], preferred_element_type=jnp.float32)
        hidden = jax.nn.silu(gate_part) * up_part
        pieces.append(jnp.where((row_expert == expert)[:, None], hidden, 0.0).astype(jnp.bfloat16))
    hidden = jnp.concatenate(pieces, axis=1)
    down = expert_down.reshape(hidden.shape[1], model_width)
    part = jnp.dot(hidden, down, preferred_element_type=jnp.float32).astype(jnp.bfloat16)
    part = part.reshape(tp_size, ep_size, block_slots, model_width)
    shared_term = shared_term_of(own_all, shared_gate, shared_up, shared_down).reshape(
        tp_size, row_count, model_width
    )
    mixer_term = mixer_term.reshape(tp_size, shard_rows // tp_size, model_width)
    back_rows, shared_sum, mixer_sum = back_exchange(
        ep_size, tp_size, part, shared_term, mixer_term
    )
    back_rows = back_rows.reshape(slot_total, model_width)
    placed = slot_index[:, :, None] == slots[None, None, :]
    mixing = jnp.sum(jnp.where(placed, route_weights[:, :, None], 0.0), axis=1)
    mixing_high = mixing.astype(jnp.bfloat16)
    mixing_low = (mixing - mixing_high.astype(jnp.float32)).astype(jnp.bfloat16)
    routed = jnp.dot(mixing_high, back_rows, preferred_element_type=jnp.float32) + jnp.dot(
        mixing_low, back_rows, preferred_element_type=jnp.float32
    )
    combined = routed + shared_sum
    expert_out = root_norm(combined, exit_gain).astype(jnp.bfloat16)
    mixer_out = root_norm(mixer_sum, mixer_gain).astype(jnp.bfloat16)
    return (mixer_out, expert_out)


def solution(mesh):
    in_specs = (
        P("ep", "tp"),
        P("ep", "tp"),
        P("ep", "tp"),
        P("ep", "tp"),
        P("tp", None),
        P(),
        P(("ep", "tp"), None),
        P(),
        P(("ep", "tp"), None),
        P(("ep", "tp"), None),
        P("ep", None, "tp"),
        P("ep", None, "tp"),
        P("ep", "tp", None),
        P(None, "tp"),
        P(None, "tp"),
        P("tp", None),
        P(),
    )
    out_specs = (P(("ep", "tp"), None), P(("ep", "tp"), None))
    return jax.shard_map(
        on_device, mesh=mesh, in_specs=in_specs, out_specs=out_specs, check_vma=False
    )
```

time: 288 us -> 208 us (0.72)
  Pallas kernels: 0 us -> 145 us
  blocking collectives: 102 us -> 0 us
  waiting for transfers between devices: 91.6 us -> 0 us
  between operations: 14.4 us -> 0.89 us
  starting transfers between devices: 13.5 us -> 0 us
  other arithmetic: 24.1 us -> 16.3 us
  matrix products: 30.9 us -> 34 us
    pallas_call x0 -> x2, Pallas kernels: none -> 145 us  [the longest x1 85.5 us: back_exchange(): pl.pallas_call(functools.partial(back_kernel, ep_size, tp_size), out_shap...]
    all_gather x3 -> x0, blocking collectives: 102 us -> none  [the longest x1 39.9 us: on_device(): lax.all_gather(key_bias, 'ep', axis=0, tiled=True)]
    all_gather x4 -> x0, waiting for transfers between devices: 55.2 us -> none  [the longest x1 53.5 us: on_device(): lax.all_gather(expert_down, 'tp', axis=1, tiled=True)]
    all_to_all x2 -> x0, waiting for transfers between devices: 30.1 us -> none  [the longest x1 30.1 us: on_device(): lax.all_to_all(returned_rows, 'ep', split_axis=0, concat_axis=0, tiled=True)]
    all_to_all x2 -> x0, starting transfers between devices: 13.1 us -> none  [the longest x1 7.45 us: on_device(): lax.all_to_all(outgoing, 'ep', split_axis=0, concat_axis=0, tiled=True)]
    reduce_sum x2 -> x1, other arithmetic: 6.75 us -> 0.12 us  [on_device(): mixing = jnp.sum(jnp.where(placed, route_weights[:, :, None], 0.0), axis=1)]
    reduce_scatter x2 -> x0, waiting for transfers between devices: 4.42 us -> none  [the longest x1 4.4 us: on_device(): lax.psum_scatter(mixer_term.astype(jnp.bfloat16), 'tp', scatter_dimension...]
    reshape x4 -> x1, local copies, waits for them, and re-layouts: 4.53 us -> 0.72 us  [on_device(): jnp.swapaxes(bias_all[:, :head_count, :], 1, 2)]
  transfers between devices with their start and end apart: 8 -> 0, of which waited for: 4 -> 0; matrix products, arithmetic and copies ran while one was open for 21% -> 0% of each run, Pallas kernels for 0% -> 0%
where the time goes in v1:
time: 208 us
  Pallas kernels  145 us (70%)
  matrix products  34 us (16%)
  other arithmetic  16.3 us (8%)
  local copies, waits for them, and re-layouts  11.8 us (6%)
    pallas_call x1, Pallas kernels, back_exchange(): pl.pallas_call(functools.partial(back_kernel, ep_size, tp_size), out_shap...  85.5 us
    pallas_call x1, Pallas kernels, front_exchange(): pl.pallas_call(functools.partial(front_kernel, ep_size, tp_size), out_sha...  59 us
    dot_general x2, matrix products, on_device(): jnp.dot(rows, expert_gate[expert], preferred_element_type=jnp.float32)  6.88 us
    another operation x6, other arithmetic  5.54 us
    dot_general x1, matrix products, on_device(): jnp.dot(hidden, down, preferred_element_type=jnp.float32)  5.42 us
    dot_general x1, matrix products, shared_term_of(): jnp.dot(hidden, shared_down, preferred_element_type=jnp.float32)  5.07 us
    dot_general x2, matrix products, on_device(): jnp.dot(rows, expert_up[expert], preferred_element_type=jnp.float32)  4.16 us

profile of v1, /device:TPU:0, one launch (start us, length us, event | category | flops | bytes accessed | tf_op | source)
XLA Modules:
  0.0 207.6 jit_solution(4214722709406065698)
XLA Ops:
  0.7 1.6 copy-done
  2.2 1.5 pad_maximum_fusion.kv_ref
  3.8 1.3 pad.8.bias_ref
  5.0 1.2 fusion.35
  6.2 1.2 fusion.37.normed_ref
  7.4 0.8 copy.66
  8.2 0.1 eq.69
  8.4 0.6 reduce-window.14
  9.0 0.2 slice_reduce_fusion
  9.2 0.1 bitcast_bitcast_fusion
  9.3 0.1 reduce_sum.58
  9.5 0.1 fusion.43
  9.6 1.8 convolution_convert_fusion.2
  11.4 59.0 %front_exchange.1 = (bf16[8,128,512]{2,1,0:T(8,128)(2,1)}, bf16[8,16,128]{2,1,0:T(8,128)(2,1)}, bf16[4,96,2048]{2,1,0:T(8,128)(2,1)}, bf16[4,8,48,2048]{3,2,1,0:T(8,128)(2,1)}) custom-call(bf16[128,512]{1,0:T(8,128)(2,1)} %pad_maximum_fusion.kv_ref, bf16[16,128]{1,0:T(8,128)(2,1)} %pad.8.bias_ref, bf16[96,2048]{1,0:T(8,128)(2,1)} %copy-done.5, ...), custom_call_target="tpu_custom_call" | custom-call | tf_op jit(solution)/shard_map/front_exchange/pallas_call | solution.py:202
  70.5 5.0 %fusion.26 = f32[1536,256]{0,1:T(8,128)S(1)} fusion(bf16[1536,2048]{1,0:T(8,128)(2,1)} %bitcast.117, bf16[2,2048,256]{2,1,0:T(8,128)(2,1)} %param.29), kind=kOutput, calls=%fused_computation.46 | convolution fusion | flops 1610612736 | bytes 8912896 | tf_op jit(solution)/shard_map/dot_general | solution.py:541
  75.6 0.4 copy-done.14
  76.0 2.1 %fusion.18 = bf16[1536,256]{0,1:T(8,128)(2,1)S(1)} fusion(bf16[1536,2048]{1,0:T(8,128)(2,1)S(1)} %bitcast.118, f32[1536,256]{0,1:T(8,128)S(1)} %fusion.26, bf16[2,2048,256]{2,1,0:T(8,128)(2,1)S(1)} %copy-done.14, pred[1536]{0:T(1024)(128)(4,1)S(1)} %broadcast_compare_fusion.1), kind=kOutput, calls=%fused_computation.35 | convolution fusion | flops 1613365248 | bytes 9701376 | tf_op jit(solution)/shard_map/dot_general | solution.py:542
  78.1 1.9 fusion.29
  80.0 2.1 %fusion.19 = bf16[1536,256]{0,1:T(8,128)(2,1)S(1)} fusion(bf16[1536,2048]{1,0:T(8,128)(2,1)S(1)} %bitcast.120, f32[1536,256]{0,1:T(8,128)S(1)} %fusion.29, bf16[2,2048,256]{2,1,0:T(8,128)(2,1)S(1)} %copy-done.14, pred[1536]{0:T(1024)(128)(4,1)S(1)} %broadcast_compare_fusion.2), kind=kOutput, calls=%fused_computation.36 | convolution fusion | flops 1613365248 | bytes 9701376 | tf_op jit(solution)/shard_map/dot_general | solution.py:542
  82.1 5.4 %convolution_convert_fusion = bf16[1536,2048]{1,0:T(8,128)(2,1)} fusion(bf16[512,2048]{1,0:T(8,128)(2,1)S(1)} %bitcast.102, bf16[1536,256]{0,1:T(8,128)(2,1)S(1)} %fusion.18, bf16[1536,256]{0,1:T(8,128)(2,1)S(1)} %fusion.19), kind=kOutput, calls=%fused_computation.28 | convolution fusion | flops 3227516928 | bytes 9961472 | tf_op jit(solution)/shard_map/dot_general | solution.py:547
  87.5 1.3 fusion.60
  88.9 5.1 %convolution_convert_fusion.1 = bf16[384,2048]{1,0:T(8,128)(2,1)} fusion(bf16[256,2048]{1,0:T(8,128)(2,1)} %param.34, bf16[384,2048]{1,0:T(8,128)(2,1)} %bitcast.121, bf16[2048,256]{1,0:T(8,128)(2,1)} %param.33, f32[384,256]{1,0:T(8,128)} %fusion.60), kind=kOutput, calls=%fused_computation.29 | convolution fusion | flops 806682624 | bytes 5636096 | tf_op jit(solution)/shard_map/dot_general | solution.py:447
  93.9 2.2 %fusion.59 = (bf16[8,128,256]{2,1,0:T(8,128)(2,1)S(1)}, bf16[8,128,256]{2,1,0:T(8,128)(2,1)}) fusion(bf16[8,128,512]{2,1,0:T(8,128)(2,1)} %get-tuple-element.64), kind=kLoop, calls=%fused_computation.114 | loop fusion | bytes 2097152 | tf_op jit(solution)/shard_map/slice | solution.py:510
  96.1 0.7 copy.70
  96.8 0.7 slice_bitcast_fusion.1
  97.6 0.7 broadcast_in_dim.70
  98.2 14.1 %while.13 = (s32[]{:T(128)}, f32[128,4,64]{0,2,1:T(8,128)}, f32[4,128]{1,0:T(4,128)S(1)}, s32[]{:T(128)}, s32[]{:T(128)}, /*index=5*/bf16[1024,256]{1,0:T(8,128)...) while((s32[]{:T(128)}, f32[128,4,64]{0,2,1:T(8,128)}, ...), condition=%wide.region_9.10_spmd.clone, body=%wide.region_5.9_spmd.clone.sunk | while | flops 109160584 | bytes 23164216 | solution.py:532
  98.2 1.1 constant_dynamic-slice_fusion.3
  99.4 0.1 copy.87
  99.6 0.1 broadcast_compare_fusion.4
  99.7 0.1 copy.88
  99.9 2.9 %fusion.95 = (f32[4,128]{1,0:T(4,128)S(1)}, f32[4,128,512]{1,2,0:T(8,128)S(1)}, f32[4,128,512]{1,2,0:T(8,128)}) fusion(pred[128,512]{0,1:T(8,128)(4,1)S(1)} %broadcast_compare_fusion.4, f32[4,512]{1,0:T(4,128)S(1)} %convert_bitcast_fusion.4, bf16[512,4,64]{0,2,1:T(8,128)(2,1)S(1)} %bitcast.105, bf16[128,4,64]{0,2,1:T(8,128)(2,1)} %get-tuple-element.272), kind=kOutput, calls=%fused_computation.27.clone.1 | convolution fusion | flops 36437504 | bytes 2500608 | tf_op jit(solution)/shard_map/while/body/qhd,khd->hqk/dot_general | solution.py:423
  102.7 4.8 %fusion.96 = f32[4,128,4,128]{1,2,3,0:T(4,128)S(1)} fusion(f32[4,128,4,128]{1,3,2,0:T(8,128)S(1)} %bitcast.103), kind=kOutput, calls=%fused_computation.17.clone.1 | output fusion | flops 33292288 | bytes 2097152 | tf_op jit(solution)/shard_map/reduce-window
  107.6 0.2 broadcast_add_fusion.2
  107.8 0.1 copy.89
  107.9 1.1 copy-done.1
  109.0 1.5 fusion.97
  110.5 1.8 fusion.98
  112.3 0.9 convert_element_type.68
  113.2 2.4 %convolution_convert_fusion.3 = bf16[128,2048]{1,0:T(8,128)(2,1)} fusion(bf16[128,256]{0,1:T(8,128)(2,1)S(1)} %bitcast.114, bf16[256,2048]{1,0:T(8,128)(2,1)} %param.23), kind=kOutput, calls=%fused_computation.37 | convolution fusion | flops 134479872 | bytes 1638400 | tf_op jit(solution)/shard_map/dot_general | solution.py:534
  115.6 85.5 %back_exchange.1 = (bf16[8,48,2048]{2,1,0:T(8,128)(2,1)}, f32[96,2048]{1,0:T(8,128)}, f32[32,2048]{1,0:T(8,128)}) custom-call(bf16[4,8,48,2048]{3,2,1,0:T(8,128)(2,1)} %bitcast.110, bf16[4,96,2048]{2,1,0:T(8,128)(2,1)} %bitcast.113, bf16[4,32,2048]{2,1,0:T(8,128)(2,1)} %bitcast.112), custom_call_target="tpu_custom_call" | custom-call | tf_op jit(solution)/shard_map/back_exchange/pallas_call | solution.py:370
  201.1 1.1 multiply_reduce_fusion.1
  202.2 1.8 multiply_convert_fusion.1
  204.1 0.1 select_reduce_fusion
  204.2 1.8 fusion.46
  206.1 0.5 multiply_reduce_fusion
  206.6 0.1 copy-done.8
  206.7 0.9 multiply_convert_fusion
  (50 shorter events, 0.4 us)
Async XLA Ops:
  0.6 1.6 copy-start
  0.6 8.9 %copy-start.10 = (s32[96,2]{0,1:T(2,128)S(1)}, s32[96,2]{0,1:T(2,128)}, u32[]{:S(2)}) copy-start(s32[96,2]{0,1:T(2,128)} %param.27) | copy-start | bytes 2308
  7.4 4.0 %copy-start.5 = (bf16[96,2048]{1,0:T(8,128)(2,1)}, bf16[96,2048]{1,0:T(8,128)(2,1)S(1)}, u32[]{:S(2)}) copy-start(bf16[96,2048]{1,0:T(8,128)(2,1)S(1)} %fusion.37.normed_ref) | copy-start | bytes 1179652
  70.5 5.1 %copy-start.12 = (bf16[4,8,48,2048]{3,2,1,0:T(8,128)(2,1)S(1)}, bf16[4,8,48,2048]{3,2,1,0:T(8,128)(2,1)}, u32[]{:S(2)}) copy-start(bf16[4,8,48,2048]{3,2,1,0:T(8,128)(2,1)} %get-tuple-element.62) | copy-start | bytes 18874372
  70.5 5.5 %copy-start.14 = (bf16[2,2048,256]{2,1,0:T(8,128)(2,1)S(1)}, bf16[2,2048,256]{2,1,0:T(8,128)(2,1)}, u32[]{:S(2)}) copy-start(bf16[2,2048,256]{2,1,0:T(8,128)(2,1)} %param.30) | copy-start | bytes 6291460
  76.0 2.1 %copy-start.13 = (bf16[2,2048,256]{2,1,0:T(8,128)(2,1)S(1)}, bf16[2,2048,256]{2,1,0:T(8,128)(2,1)}, u32[]{:S(2)}) copy-start(bf16[2,2048,256]{2,1,0:T(8,128)(2,1)} %param.29) | copy-start | bytes 6291460
  82.1 5.4 %copy-start.15 = (bf16[4,96,2048]{2,1,0:T(8,128)(2,1)S(1)}, bf16[4,96,2048]{2,1,0:T(8,128)(2,1)}, u32[]{:S(2)}) copy-start(bf16[4,96,2048]{2,1,0:T(8,128)(2,1)} %get-tuple-element.63) | copy-start | bytes 4718596
  82.1 5.4 %copy-start.16 = (bf16[2048,256]{1,0:T(8,128)(2,1)S(1)}, bf16[2048,256]{1,0:T(8,128)(2,1)}, u32[]{:S(2)}) copy-start(bf16[2048,256]{1,0:T(8,128)(2,1)} %param.32) | copy-start | bytes 3145732
  93.9 2.2 %copy-start.7 = (bf16[128,256]{1,0:T(8,128)(2,1)S(1)}, bf16[128,256]{1,0:T(8,128)(2,1)}, u32[]{:S(2)}) copy-start(bf16[128,256]{1,0:T(8,128)(2,1)} %param.19) | copy-start | bytes 196612
  98.2 4.5 %copy-start.2 = (bf16[1024,256]{1,0:T(8,128)(2,1)}, bf16[1024,256]{1,0:T(8,128)(2,1)S(1)}, u32[]{:S(2)}) copy-start(bf16[1024,256]{1,0:T(8,128)(2,1)S(1)} %get-tuple-element.271) | copy-start | bytes 1572868 | tf_op jit(solution)/shard_map/while
  107.8 1.2 copy-start.1
  109.0 3.3 %copy-start.3 = (bf16[1024,256]{1,0:T(8,128)(2,1)S(1)}, bf16[1024,256]{1,0:T(8,128)(2,1)}, u32[]{:S(2)}) copy-start(bf16[1024,256]{1,0:T(8,128)(2,1)} %copy-done.2) | copy-start | bytes 1572868 | tf_op jit(solution)/shard_map/while
  115.6 86.6 %copy-start.9 = (f32[2048]{0:T(1024)S(1)}, f32[2048]{0:T(1024)}, u32[]{:S(2)}) copy-start(f32[2048]{0:T(1024)} %param.24) | copy-start | bytes 24580
  115.6 88.5 %copy-start.11 = (f32[96,2]{0,1:T(2,128)S(1)}, f32[96,2]{0,1:T(2,128)}, u32[]{:S(2)}) copy-start(f32[96,2]{0,1:T(2,128)} %param.28) | copy-start | bytes 2308
  202.2 3.9 %copy-start.4 = (bf16[8,48,2048]{2,1,0:T(8,128)(2,1)S(1)}, bf16[8,48,2048]{2,1,0:T(8,128)(2,1)}, u32[]{:S(2)}) copy-start(bf16[8,48,2048]{2,1,0:T(8,128)(2,1)} %get-tuple-element.68) | copy-start | bytes 4718596
  202.2 3.9 %copy-start.6 = (f32[96,2048]{1,0:T(8,128)S(1)}, f32[96,2048]{1,0:T(8,128)}, u32[]{:S(2)}) copy-start(f32[96,2048]{1,0:T(8,128)} %get-tuple-element.69) | copy-start | bytes 2359300
  206.0 0.7 copy-start.8

commit v2 on v1

--- a/solution.py
+++ b/solution.py
@@ -46,20 +46,24 @@
 def front_kernel(
     ep_size,
     tp_size,
+    head_size,
+    query_ref,
     kv_ref,
-    bias_ref,
     normed_ref,
     outgoing_ref,
-    kv_all,
-    bias_all,
+    attended_ref,
     own_all,
     arrived,
+    kv_all,
+    query_heads,
+    carried,
+    output,
     ep_send,
     ep_recv,
     kv_send,
     kv_recv,
-    bias_send,
-    bias_recv,
+    pair_send,
+    pair_recv,
     partner_send,
     partner_recv,
     across_send,
@@ -88,25 +92,67 @@
         block = arrived.at[own_tp, source]
         return send_of(block, block, ep_send.at[step], ep_recv.at[step], (own_ep, own_tp))
 
+    shard_rows, width = query_ref.shape
+    head_count = width // head_size
+    lines = ep_size // 2
+    parity = lax.rem(own_ep, 2)
+    own_line = own_ep // 2
+    pair_ep = own_ep + 1 - 2 * parity
+
     def spread_kv(step):
-        target = lax.rem(own_ep + step, ep_size)
+        target = 2 * lax.rem(own_line + step, lines) + parity
         return send_of(
             kv_ref, kv_all.at[own_ep], kv_send.at[step], kv_recv.at[step], (target, own_tp)
         )
 
+    def line_kv(step, side):
+        return kv_all.at[2 * lax.rem(own_line - step + lines, lines) + side]
+
     def landed_kv(step):
-        block = kv_all.at[lax.rem(own_ep - step + ep_size, ep_size)]
+        block = line_kv(step, parity)
         return send_of(block, block, kv_send.at[step], kv_recv.at[step], (own_ep, own_tp))
 
-    def spread_bias(step):
-        target = lax.rem(own_ep + step, ep_size)
+    def pair_kv(source, target, step):
         return send_of(
-            bias_ref, bias_all.at[own_ep], bias_send.at[step], bias_recv.at[step], (target, own_tp)
+            source, target, pair_send.at[step], pair_recv.at[step], (pair_ep, own_tp)
         )
 
-    def landed_bias(step):
-        block = bias_all.at[lax.rem(own_ep - step + ep_size, ep_size)]
-        return send_of(block, block, bias_send.at[step], bias_recv.at[step], (own_ep, own_tp))
+    def attend_block(keys_values, own):
+        keys = keys_values[0:shard_rows, 0:width]
+        values = keys_values[0:shard_rows, width : 2 * width]
+        ahead = lax.broadcasted_iota(jnp.int32, (shard_rows, shard_rows), 0)
+        behind = lax.broadcasted_iota(jnp.int32, (shard_rows, shard_rows), 1)
+        later_of = jnp.where(ahead > behind, 1.0, 0.0)
+        column_head = lax.broadcasted_iota(jnp.int32, (shard_rows, width), 1) // head_size
+        gained = jnp.zeros((shard_rows, width), jnp.float32)
+        for head in range(head_count):
+            bias_row = keys_values[shard_rows + head : shard_rows + head + 1, 0:shard_rows]
+            scores = lax.dot_general(
+                query_heads[head],
+                keys,
+                (((1,), (1,)), ((), ())),
+                preferred_element_type=jnp.float32,
+            )
+            scores = scores * head_size ** (-0.5) + bias_row.astype(jnp.float32)
+            tail = jnp.log1p(jnp.exp(-jnp.abs(scores)))
+            fails = -(jnp.maximum(scores, 0.0) + tail)
+            if own:
+                fails = jnp.where(behind < ahead, fails, 0.0)
+            later = jnp.dot(
+                fails,
+                later_of,
+                preferred_element_type=jnp.float32,
+                precision=lax.Precision.HIGHEST,
+            )
+            weights = jnp.exp(jnp.minimum(scores, 0.0) - tail + later + carried[head])
+            if own:
+                weights = jnp.where(behind < ahead, weights, 0.0)
+            product = jnp.dot(
+                weights.astype(jnp.bfloat16), values, preferred_element_type=jnp.float32
+            )
+            gained = jnp.where(column_head == head, product, gained)
+            carried[head] = carried[head] + jnp.sum(fails, axis=1, keepdims=True)
+        output[...] = output[...] + gained
 
     def tp_block(holder, step):
         return arrived.at[holder, lax.rem(own_ep - step + ep_size, ep_size)]
@@ -119,6 +165,8 @@
     relay_sems = (relay_send, relay_recv)
     last = ep_size
 
+    lax.fori_loop(1, lines, lambda step, c: (spread_kv(step).start(), c)[1], 0)
+    pair_kv(kv_ref, kv_all.at[own_ep], 0).start()
     lax.fori_loop(1, ep_size, lambda step, c: (dispatch(step).start(), c)[1], 0)
     own_block = outgoing_ref.at[own_ep]
     own_slot = arrived.at[own_tp, own_ep]
@@ -129,27 +177,47 @@
     locals_ = [
         pltpu.make_async_copy(own_block, own_slot, local_sem.at[0]),
         pltpu.make_async_copy(normed_ref, own_all.at[own_tp], local_sem.at[1]),
-        pltpu.make_async_copy(kv_ref, kv_all.at[own_ep], local_sem.at[2]),
-        pltpu.make_async_copy(bias_ref, bias_all.at[own_ep], local_sem.at[3]),
     ]
     for local in locals_:
         local.start()
 
-    def start_kv(step, carry):
-        spread_kv(step).start()
-        spread_bias(step).start()
-        return carry
-
-    lax.fori_loop(1, ep_size, start_kv, 0)
+    output[...] = jnp.zeros_like(output)
+    carried[...] = jnp.zeros_like(carried)
+    head_of = lax.broadcasted_iota(jnp.int32, (shard_rows, width), 1) // head_size
+    queries = query_ref[...].astype(jnp.float32)
+    for head in range(head_count):
+        query_heads[head] = jnp.where(head_of == head, queries, 0.0).astype(jnp.bfloat16)
+    attend_block(kv_ref[...], True)
+
+    def relay_kv(step, carry):
+        landed_kv(step).wait_recv()
+        block = line_kv(step, parity)
+        pair_kv(block, block, step).start()
+        return carry
+
+    lax.fori_loop(1, lines, relay_kv, 0)
+
+    def landed_pair(step, carry):
+        block = line_kv(step, 1 - parity)
+        pair_kv(block, block, step).wait_recv()
+        return carry
+
+    lax.fori_loop(0, lines, landed_pair, 0)
 
     def forward(step, carry):
         landed(step).wait_recv()
         block = tp_block(own_tp, step)
         tp_copy(block, block, across_sems, step, to_across).start()
         tp_copy(block, block, partner_sems, step, to_partner).start()
+
+        @pl.when(step <= own_ep)
+        def attend_earlier():
+            attend_block(kv_all[lax.rem(own_ep - step + ep_size, ep_size)], False)
+
         return carry
 
     lax.fori_loop(1, ep_size, forward, 0)
+    attended_ref[...] = output[...].astype(jnp.bfloat16)
 
     other_own = own_all.at[across]
     tp_copy(other_own, other_own, across_sems, last, to_across).wait_recv()
@@ -182,37 +250,86 @@
 
     def finish_ep(step, carry):
         dispatch(step).wait_send()
-        spread_kv(step).wait_send()
-        spread_bias(step).wait_send()
-        landed_kv(step).wait_recv()
-        landed_bias(step).wait_recv()
         return carry
 
     lax.fori_loop(1, ep_size, finish_ep, 0)
+
+    def finish_kv(step, carry):
+        block = line_kv(step, parity)
+        pair_kv(block, block, step).wait_send()
+        return carry
+
+    lax.fori_loop(1, lines, finish_kv, 0)
+    lax.fori_loop(1, lines, lambda step, c: (spread_kv(step).wait_send(), c)[1], 0)
+    pair_kv(kv_ref, kv_all.at[own_ep], 0).wait_send()
     for local in locals_:
         local.wait()
 
 
-def front_exchange(ep_size, tp_size, kv, bias, normed, outgoing):
+def front_exchange(ep_size, tp_size, head_size, queries, kv, normed, outgoing):
     def spread(count, value):
         return jax.ShapeDtypeStruct((count,) + value.shape, value.dtype)
 
+    rows, width = queries.shape
+    heads = width // head_size
     ep_sem = pltpu.SemaphoreType.DMA((ep_size,))
     tp_sem = pltpu.SemaphoreType.DMA((ep_size + 1,))
+    vmem = pl.BlockSpec(memory_space=pltpu.VMEM)
     return pl.pallas_call(
-        functools.partial(front_kernel, ep_size, tp_size),
+        functools.partial(front_kernel, ep_size, tp_size, head_size),
         out_shape=(
-            spread(ep_size, kv),
-            spread(ep_size, bias),
+            jax.ShapeDtypeStruct(queries.shape, jnp.bfloat16),
             spread(tp_size, normed),
             spread(tp_size, outgoing),
         ),
-        in_specs=[pl.BlockSpec(memory_space=pltpu.VMEM)] * 4,
-        out_specs=[pl.BlockSpec(memory_space=pl.ANY)] * 4,
-        scratch_shapes=[ep_sem] * 6 + [tp_sem] * 6 + [pltpu.SemaphoreType.DMA((4,))],
-        compiler_params=pltpu.CompilerParams(collective_id=0, has_side_effects=True),
+        in_specs=[vmem] * 4,
+        out_specs=[vmem] + [pl.BlockSpec(memory_space=pl.ANY)] * 2,
+        scratch_shapes=[
+            pltpu.VMEM((ep_size,) + kv.shape, kv.dtype),
+            pltpu.VMEM((heads, rows, width), jnp.bfloat16),
+            pltpu.VMEM((heads, rows, 1), jnp.float32),
+            pltpu.VMEM((rows, width), jnp.float32),
+        ]
+        + [ep_sem] * 6
+        + [tp_sem] * 6
+        + [pltpu.SemaphoreType.DMA((2,))],
+        compiler_params=pltpu.CompilerParams(
+            collective_id=0, has_side_effects=True, vmem_limit_bytes=48 * 1024 * 1024
+        ),
         name="front_exchange",
-    )(kv, bias, normed, outgoing)
+    )(queries, kv, normed, outgoing)
+
+
+def expert_kernel(capacity, block_slots, rows_ref, gate_ref, up_ref, down_ref, part_ref):
+    rows = rows_ref[...]
+    row_expert = (
+        lax.rem(lax.broadcasted_iota(jnp.int32, (rows.shape[0], 1), 0), block_slots) // capacity
+    )
+    total = jnp.zeros(part_ref.shape, jnp.float32)
+    for expert in range(gate_ref.shape[0]):
+        gate = jnp.dot(rows, gate_ref[expert], preferred_element_type=jnp.float32)
+        up = jnp.dot(rows, up_ref[expert], preferred_element_type=jnp.float32)
+        hidden = gate / (1.0 + jnp.exp(-gate)) * up
+        hidden = jnp.where(row_expert == expert, hidden, 0.0).astype(jnp.bfloat16)
+        total = total + jnp.dot(hidden, down_ref[expert], preferred_element_type=jnp.float32)
+    part_ref[...] = total.astype(jnp.bfloat16)
+
+
+def expert_parts(capacity, block_slots, tile, rows, gate, up, down):
+    row_total, width = rows.shape
+
+    def whole(value):
+        return pl.BlockSpec(value.shape, lambda i: (0, 0, 0))
+
+    return pl.pallas_call(
+        functools.partial(expert_kernel, capacity, block_slots),
+        grid=(row_total // tile,),
+        out_shape=jax.ShapeDtypeStruct((row_total, width), jnp.bfloat16),
+        in_specs=[pl.BlockSpec((tile, width), lambda i: (i, 0)), whole(gate), whole(up), whole(down)],
+        out_specs=pl.BlockSpec((tile, width), lambda i: (i, 0)),
+        compiler_params=pltpu.CompilerParams(vmem_limit_bytes=60 * 1024 * 1024),
+        name="expert_parts",
+    )(rows, gate, up, down)
 
 
 def back_kernel(
@@ -409,37 +526,6 @@
     return values * lax.rsqrt(jnp.mean(values * values, axis=-1, keepdims=True) + EPS) * gain_row
 
 
-def block_shards(shard_rows, ep_size):
-    shards = 1
-    while shards * shard_rows < 512 and ep_size % (2 * shards) == 0:
-        shards = shards * 2
-    return shards
-
-
-def break_scores(query_split, block_keys, block_bias, query_pos, key_start):
-    head_count = query_split.shape[1]
-    key_count = block_keys.shape[0]
-    keys_split = block_keys.reshape(key_count, head_count, query_split.shape[2])
-    scores = jnp.einsum("qhd,khd->hqk", query_split, keys_split, preferred_element_type=jnp.float32)
-    scores = (
-        scores * query_split.shape[2] ** (-0.5)
-        + jnp.transpose(block_bias.astype(jnp.float32))[:, None, :]
-    )
-    key_pos = key_start + jnp.arange(key_count, dtype=jnp.int32)
-    causal = (key_pos[None, :] < query_pos[:, None])[None]
-    fail_logs = jnp.where(causal, -jax.nn.softplus(scores), 0.0)
-    return (scores, fail_logs, causal)
-
-
-def break_values(scores, fail_logs, causal, offset, block_values):
-    later_sum = lax.cumsum(fail_logs, axis=2, reverse=True) - fail_logs + offset[:, :, None]
-    weights = jnp.where(causal, jnp.exp(jax.nn.log_sigmoid(scores) + later_sum), 0.0).astype(
-        jnp.bfloat16
-    )
-    values_split = block_values.reshape(block_values.shape[0], scores.shape[0], -1)
-    return jnp.einsum("hqk,khd->qhd", weights, values_split, preferred_element_type=jnp.float32)
-
-
 def shared_term_of(own_all, shared_gate, shared_up, shared_down):
     gate_part = jnp.dot(own_all, shared_gate, preferred_element_type=jnp.float32)
     up_part = jnp.dot(own_all, shared_up, preferred_element_type=jnp.float32)
@@ -471,18 +557,13 @@
     head_size = query_rows.shape[1] // head_count
     ep_size = lax.axis_size("ep")
     tp_size = lax.axis_size("tp")
-    own_index = lax.axis_index("ep")
-    query_split = query_rows.reshape(shard_rows, head_count, head_size)
-    query_pos = own_index * shard_rows + jnp.arange(shard_rows, dtype=jnp.int32)
-    span_shards = block_shards(shard_rows, ep_size)
-    empty_output = jnp.zeros((shard_rows, head_count, head_size), jnp.float32)
     row_count = routed_input.shape[0]
     local_experts = expert_gate.shape[0]
     model_width = routed_input.shape[1]
     expert_count = local_experts * ep_size
     top_count = expert_index.shape[1]
     capacity = 3 * row_count * top_count // (2 * expert_count)
-    block_slots = -(-local_experts * capacity // 16) * 16
+    block_slots = -(-local_experts * capacity // 8) * 8
     slot_total = ep_size * block_slots
     normed = root_norm(routed_input.astype(jnp.float32), entry_gain).astype(jnp.bfloat16)
     flat_expert = expert_index.reshape(-1)
@@ -501,50 +582,27 @@
     outgoing = jnp.dot(selector, normed, preferred_element_type=jnp.float32).astype(jnp.bfloat16)
     outgoing = outgoing.reshape(ep_size, block_slots, model_width)
     bias_rows = -(-head_count // 16) * 16
-    bias_block = jnp.pad(jnp.transpose(key_bias), ((0, bias_rows - head_count), (0, 0)))
-    kv_block = jnp.concatenate([key_rows, value_rows], axis=1)
-    kv_all, bias_all, own_all, arrived = front_exchange(
-        ep_size, tp_size, kv_block, bias_block, normed, outgoing
-    )
-    width = key_rows.shape[1]
-    all_keys = kv_all[:, :, :width].reshape(ep_size * shard_rows, width)
-    all_values = kv_all[:, :, width:].reshape(ep_size * shard_rows, width)
-    all_bias = jnp.swapaxes(bias_all[:, :head_count, :], 1, 2).reshape(
-        ep_size * shard_rows, head_count
+    bias_block = jnp.pad(
+        jnp.transpose(key_bias),
+        ((0, bias_rows - head_count), (0, 2 * key_rows.shape[1] - shard_rows)),
+    )
+    kv_block = jnp.concatenate(
+        [jnp.concatenate([key_rows, value_rows], axis=1), bias_block], axis=0
+    )
+    attended, own_all, arrived = front_exchange(
+        ep_size, tp_size, head_size, query_rows, kv_block, normed, outgoing
     )
     own_all = own_all.reshape(tp_size * row_count, model_width)
-    block_rows = span_shards * shard_rows
-    own_block = own_index * shard_rows // block_rows
-
-    def backward_turn(turn_index, carried_pair):
-        output, carried = carried_pair
-        block_start = (own_block - turn_index) * block_rows
-        block_keys = lax.dynamic_slice_in_dim(all_keys, block_start, block_rows, 0)
-        block_values = lax.dynamic_slice_in_dim(all_values, block_start, block_rows, 0)
-        block_bias = lax.dynamic_slice_in_dim(all_bias, block_start, block_rows, 0)
-        scores, fail_logs, causal = break_scores(
-            query_split, block_keys, block_bias, query_pos, block_start
-        )
-        output = output + break_values(scores, fail_logs, causal, carried, block_values)
-        return (output, carried + jnp.sum(fail_logs, axis=2))
-
-    carried_zero = jnp.zeros((head_count, shard_rows), jnp.float32)
-    output, unused = lax.fori_loop(0, own_block + 1, backward_turn, (empty_output, carried_zero))
-    attended = output.reshape(shard_rows, head_count * head_size).astype(jnp.bfloat16)
     mixer_term = jnp.dot(attended, mixer_weight, preferred_element_type=jnp.float32).astype(
         jnp.bfloat16
     )
     rows = arrived.reshape(tp_size * slot_total, model_width)
-    row_expert = jnp.arange(tp_size * slot_total, dtype=jnp.int32) % block_slots // capacity
-    pieces = []
-    for expert in range(local_experts):
-        gate_part = jnp.dot(rows, expert_gate[expert], preferred_element_type=jnp.float32)
-        up_part = jnp.dot(rows, expert_up[expert], preferred_element_type=jnp.float32)
-        hidden = jax.nn.silu(gate_part) * up_part
-        pieces.append(jnp.where((row_expert == expert)[:, None], hidden, 0.0).astype(jnp.bfloat16))
-    hidden = jnp.concatenate(pieces, axis=1)
-    down = expert_down.reshape(hidden.shape[1], model_width)
-    part = jnp.dot(hidden, down, preferred_element_type=jnp.float32).astype(jnp.bfloat16)
+    tile = slot_total
+    while tile > 384 and tile % 32 == 0:
+        tile = tile // 2
+    part = expert_parts(
+        capacity, block_slots, tile, rows, expert_gate, expert_up, expert_down
+    )
     part = part.reshape(tp_size, ep_size, block_slots, model_width)
     shared_term = shared_term_of(own_all, shared_gate, shared_up, shared_down).reshape(
         tp_size, row_count, model_width

time: 208 us -> 147 us (0.71)
  matrix products: 34 us -> 8.81 us
  Pallas kernels: 145 us -> 130 us
  other arithmetic: 16.3 us -> 5.83 us
  local copies, waits for them, and re-layouts: 11.8 us -> 1.56 us
    pallas_call x1, Pallas kernels: 85.5 us -> 56.1 us  [back_exchange(): pl.pallas_call(functools.partial(back_kernel, ep_size, tp_size), out_shap...]
    dot_general x7 -> x0, matrix products: 21.1 us -> none  [the longest x2 6.88 us: on_device(): jnp.dot(rows, expert_gate[expert], preferred_element_type=jnp.float32)]
    pallas_call x1 -> x2, Pallas kernels: 59 us -> 73.7 us  [the longest x1 59.7 us: front_exchange(): pl.pallas_call(functools.partial(front_kernel, ep_size, tp_size, head_siz...]
    another operation x7 -> x4, other arithmetic: 5.72 us -> 0.71 us
    unnamed x30 -> x27, local copies, waits for them, and re-layouts: 3.75 us -> 1.04 us
    convert_element_type x2 -> x0, other arithmetic: 2.4 us -> none  [the longest x1 1.48 us: break_values(): jnp.where(causal, jnp.exp(jax.nn.log_sigmoid(scores) + later_sum), 0.0)]
where the time goes in v2:
time: 147 us
  Pallas kernels  130 us (88%)
  matrix products  8.81 us (6%)
  other arithmetic  5.83 us (4%)
  local copies, waits for them, and re-layouts  1.56 us (1%)
    pallas_call x1, Pallas kernels, front_exchange(): pl.pallas_call(functools.partial(front_kernel, ep_size, tp_size, head_siz...  59.7 us
    pallas_call x1, Pallas kernels, back_exchange(): pl.pallas_call(functools.partial(back_kernel, ep_size, tp_size), out_shap...  56.1 us
    pallas_call x1, Pallas kernels, expert_parts(): pl.pallas_call(functools.partial(expert_kernel, capacity, block_slots), g...  14 us
    dot_general x1, matrix products, shared_term_of(): jnp.dot(hidden, shared_down, preferred_element_type=jnp.float32)  4.17 us

profile of v2, /device:TPU:0, one launch (start us, length us, event | category | flops | bytes accessed | tf_op | source)
XLA Modules:
  0.0 146.9 jit_solution(8811826840024425535)
XLA Ops:
  0.6 0.0 copy-start
  0.6 0.9 copy.45
  1.5 0.1 eq.50
  1.7 0.6 reduce-window.6
  2.3 0.0 copy-start.6
  2.3 0.0 copy-start.7
  2.3 0.0 copy-start.10
  2.3 0.2 slice_reduce_fusion
  2.5 0.1 bitcast_bitcast_fusion
  2.6 0.1 reduce_sum.49
  2.7 0.1 copy.48
  2.8 0.7 fusion.21
  3.5 0.1 fusion.10
  3.6 0.0 copy-start.1
  3.7 1.2 fusion.2
  4.9 1.2 fusion.4.normed_ref
  6.0 0.0 copy-start.12
  6.1 0.5 convolution_convert_fusion.1
  6.6 0.0 copy-done.6
  6.6 0.0 copy-done.7
  6.6 0.0 copy-done.10
  6.7 0.0 copy-done.1
  6.7 59.7 %front_exchange.1 = (bf16[128,256]{1,0:T(8,128)(2,1)S(1)}, bf16[4,96,2048]{2,1,0:T(8,128)(2,1)S(1)}, bf16[4,8,40,2048]{3,2,1,0:T(8,128)(2,1)}) custom-call(bf16[128,256]{1,0:T(8,128)(2,1)S(1)} %copy-done.1, bf16[144,512]{1,0:T(8,128)(2,1)S(1)} %fusion.13.kv_ref, bf16[96,2048]{1,0:T(8,128)(2,1)S(1)} %fusion.4.normed_ref, bf16[8,40,2048]{2,1,0:T(8,128)(2,1)S(1)} %bitcast.31), custom_call_target="tpu_custom_call" | custom-call | tf_op jit(solution)/shard_map/front_exchange/pallas_call | solution.py:278
  66.3 0.0 copy-done.12
  66.4 0.6 fusion.23
  66.9 0.0 copy-done
  67.0 4.2 %convolution_convert_fusion = bf16[384,2048]{1,0:T(8,128)(2,1)} fusion(bf16[256,2048]{1,0:T(8,128)(2,1)S(1)} %copy-done, bf16[384,2048]{1,0:T(8,128)(2,1)S(1)} %bitcast.33, bf16[2048,256]{1,0:T(8,128)(2,1)} %param.31, f32[384,256]{1,0:T(8,128)S(1)} %fusion.23), kind=kOutput, calls=%fused_computation | convolution fusion | flops 806682624 | bytes 5636096 | tf_op jit(solution)/shard_map/dot_general | solution.py:533
  71.1 14.0 %expert_parts.1 = bf16[1280,2048]{1,0:T(8,128)(2,1)} custom-call(bf16[1280,2048]{1,0:T(8,128)(2,1)} %bitcast.35, bf16[2,2048,256]{2,1,0:T(8,128)(2,1)} %gate_ref.1, bf16[2,2048,256]{2,1,0:T(8,128)(2,1)} %up_ref.1, bf16[2,256,2048]{2,1,0:T(8,128)(2,1)} %down_ref.1), custom_call_target="tpu_custom_call" | custom-call | tf_op jit(solution)/shard_map/expert_parts/pallas_call | solution.py:324
  85.2 0.0 copy-done.4
  85.2 1.1 convolution_convert_fusion.2
  86.3 56.1 %back_exchange.1 = (bf16[8,40,2048]{2,1,0:T(8,128)(2,1)}, f32[96,2048]{1,0:T(8,128)}, f32[32,2048]{1,0:T(8,128)}) custom-call(bf16[4,8,40,2048]{3,2,1,0:T(8,128)(2,1)} %bitcast.34, bf16[4,96,2048]{2,1,0:T(8,128)(2,1)} %bitcast.39, bf16[4,32,2048]{2,1,0:T(8,128)(2,1)} %bitcast.38), custom_call_target="tpu_custom_call" | custom-call | tf_op jit(solution)/shard_map/back_exchange/pallas_call | solution.py:487
  142.4 0.0 copy-start.2
  142.4 0.0 copy-start.5
  142.4 0.0 copy-done.11
  142.4 0.1 select_reduce_fusion
  142.5 1.9 %fusion.15 = f32[96,2048]{1,0:T(8,128)S(1)} fusion(bf16[320,2048]{1,0:T(8,128)(2,1)} %bitcast.36, f32[96,320]{1,0:T(8,128)S(1)} %select_reduce_fusion), kind=kOutput, calls=%fused_computation.31 | convolution fusion | flops 125859840 | bytes 2220032 | tf_op jit(solution)/shard_map/dot_general | solution.py:619
  144.4 0.0 copy-done.2
  144.4 0.0 copy-done.5
  144.4 0.0 copy-start.8
  144.4 0.0 copy-start.3
  144.4 0.0 copy-start.9
  144.5 0.5 multiply_reduce_fusion
  145.0 0.1 copy-done.8
  145.1 0.9 multiply_convert_fusion
  146.0 0.0 copy-done.3
  146.0 0.1 multiply_reduce_fusion.1
  146.1 0.0 copy-done.9
  146.1 0.8 multiply_convert_fusion.1
  (11 shorter events, 0.1 us)
Async XLA Ops:
  0.6 66.3 %copy-start = (bf16[256,2048]{1,0:T(8,128)(2,1)S(1)}, bf16[256,2048]{1,0:T(8,128)(2,1)}, u32[]{:S(2)}) copy-start(bf16[256,2048]{1,0:T(8,128)(2,1)} %param.32) | copy-start | bytes 3145732
  2.3 4.3 %copy-start.6 = (bf16[128,256]{1,0:T(8,128)(2,1)S(1)}, bf16[128,256]{1,0:T(8,128)(2,1)}, u32[]{:S(2)}) copy-start(bf16[128,256]{1,0:T(8,128)(2,1)} %param.19) | copy-start | bytes 196612
  2.3 4.4 %copy-start.7 = (bf16[128,256]{1,0:T(8,128)(2,1)S(1)}, bf16[128,256]{1,0:T(8,128)(2,1)}, u32[]{:S(2)}) copy-start(bf16[128,256]{1,0:T(8,128)(2,1)} %param.18) | copy-start | bytes 196612
  2.3 4.4 %copy-start.10 = (bf16[128,4]{0,1:T(4,128)(2,1)S(1)}, bf16[128,4]{0,1:T(4,128)(2,1)}, u32[]{:S(2)}) copy-start(bf16[128,4]{0,1:T(4,128)(2,1)} %param.20) | copy-start | bytes 3076
  3.6 3.0 %copy-start.1 = (bf16[128,256]{1,0:T(8,128)(2,1)S(1)}, bf16[128,256]{1,0:T(8,128)(2,1)}, u32[]{:S(2)}) copy-start(bf16[128,256]{1,0:T(8,128)(2,1)} %query_ref.1) | copy-start | bytes 196612
  6.0 60.3 %copy-start.12 = (bf16[2048,256]{1,0:T(8,128)(2,1)S(1)}, bf16[2048,256]{1,0:T(8,128)(2,1)}, u32[]{:S(2)}) copy-start(bf16[2048,256]{1,0:T(8,128)(2,1)} %param.30) | copy-start | bytes 3145732
  71.1 14.0 %copy-start.4 = (bf16[256,2048]{1,0:T(8,128)(2,1)S(1)}, bf16[256,2048]{1,0:T(8,128)(2,1)}, u32[]{:S(2)}) copy-start(bf16[256,2048]{1,0:T(8,128)(2,1)} %param.21) | copy-start | bytes 3145732
  86.3 56.1 %copy-start.11 = (f32[96,2]{0,1:T(2,128)S(1)}, f32[96,2]{0,1:T(2,128)}, u32[]{:S(2)}) copy-start(f32[96,2]{0,1:T(2,128)} %param.26) | copy-start | bytes 2308
  142.4 2.0 %copy-start.2 = (bf16[8,40,2048]{2,1,0:T(8,128)(2,1)S(1)}, bf16[8,40,2048]{2,1,0:T(8,128)(2,1)}, u32[]{:S(2)}) copy-start(bf16[8,40,2048]{2,1,0:T(8,128)(2,1)} %get-tuple-element.12) | copy-start | bytes 3932164
  142.4 2.0 %copy-start.5 = (f32[96,2048]{1,0:T(8,128)S(1)}, f32[96,2048]{1,0:T(8,128)}, u32[]{:S(2)}) copy-start(f32[96,2048]{1,0:T(8,128)} %get-tuple-element.13) | copy-start | bytes 2359300
  144.4 0.7 copy-start.8
  144.4 1.6 %copy-start.3 = (f32[32,2048]{1,0:T(8,128)S(1)}, f32[32,2048]{1,0:T(8,128)}, u32[]{:S(2)}) copy-start(f32[32,2048]{1,0:T(8,128)} %get-tuple-element.11) | copy-start | bytes 786436
  144.4 1.7 %copy-start.9 = (f32[2048]{0:T(1024)S(1)}, f32[2048]{0:T(1024)}, u32[]{:S(2)}) copy-start(f32[2048]{0:T(1024)} %param.22) | copy-start | bytes 24580
